TPU v7x, 256 devices: a 4x2x16 block of a 4x16x16 slice. The times are simulated.
256 devices in a mesh: grp: 2 (over y), ep: 32 (over z, core), tp: 4 (over x).
Axes of the slice: x: 4, y: 2, z: 16, core: 2. Of those that a mesh axis runs over, the one named last changes fastest.
The devices are a block of a 4x16x16 slice.
Arguments:
- query_plain: bfloat16 [16384, 512], P(('grp', 'ep'), 'tp'), parts along dimension 0, may hold values from -400 to 400
- query_rotary: bfloat16 [16384, 256], P(('grp', 'ep'), 'tp'), parts along dimension 0, may hold values from -6 to 6
- latent_input: bfloat16 [16384, 256], P(('grp', 'ep')), parts along dimension 0, may hold values from -6 to 6
- rotary_key: bfloat16 [16384, 32], P(('grp', 'ep')), parts along dimension 0, may hold values from -6 to 6
- key_weight: bfloat16 [256, 512], P(None, 'tp'), may hold values from -0.375 to 0.375
- value_weight: bfloat16 [256, 512], P(None, 'tp'), may hold values from -0.375 to 0.375
- latent_gain: bfloat16 [256], replicated, may hold values from 0.099609375 to 1.8984375
- head_gain: bfloat16 [512], P('tp'), may hold values from 0.099609375 to 1.8984375
- out_weight: bfloat16 [512, 2048], P('tp'), may hold values from -0.25 to 0.25
- expert_input: bfloat16 [32768, 2048], P(('grp', 'ep', 'tp')), parts along dimension 0, may hold values from -6 to 6
- expert_gain: bfloat16 [2048], replicated, may hold values from 0.099609375 to 1.8984375
- routes: int32 [32768, 2], P(('grp', 'ep', 'tp')), parts along dimension 0, may hold values from 0 to 31, all different within a row; in each aligned block of 128 rows (0 to 127, 128 to 255, ...) at most 9 rows name the same one
- route_weight: float32 [32768, 2], P(('grp', 'ep', 'tp')), parts along dimension 0, may hold values from 0.1 to 1
- gate_weight: bfloat16 [32, 2048, 3584], P('ep', None, 'tp'), may hold values from -0.125 to 0.125
- up_weight: bfloat16 [32, 2048, 3584], P('ep', None, 'tp'), may hold values from -0.125 to 0.125
- down_weight: bfloat16 [32, 3584, 2048], P('ep', 'tp'), may hold values from -0.09375 to 0.09375
Outputs:
- attended: bfloat16 [16384, 2048], P(('grp', 'ep', 'tp')), parts along dimension 0
- expert_out: bfloat16 [32768, 2048], P(('grp', 'ep', 'tp')), parts along dimension 0
There are 2 independent parts, one for each index of `grp`. A program takes and returns all parts, laid end to end along the dimension named above; an argument that names none is the same for every part. Nothing has to cross between parts.
Inputs may be any that keep to these rules, and one draw needn't show every extreme that they name: `routes`: each of the 128 rows of one device names 2 different experts; no expert is named by more than 9 rows of one device, a bound that some block reaches of some device.
All inputs are finite; a program needn't handle non-finite values.
Results may differ from a plain program's by a relative error of at most 0.012.
Values may be sent and summed in bfloat16 or wider, within the bound.
No kernel may reach another device: no remote copies, remote signals or barrier semaphores. Data moves between devices by JAX's collectives and lax.ppermute only.
A program may use at most 128 MiB of HBM per device.

v0:
```python
import jax
import jax.numpy as jnp
from jax import lax
from jax.sharding import Mesh
from jax.sharding import PartitionSpec as P

PLAIN_DIM = 64
ROTARY_DIM = 32
VALUE_DIM = 64
TOP = 2
EP = ("ep_0", "ep_1")
GRP_EP = ("grp", "ep_0", "ep_1")
GRP_EP_TP = ("grp", "ep_0", "ep_1", "tp")
EPSILON = 1e-06
THETA = 10000.0
key_span = 2048


def sent_together(arrays, axis, dim, along):
    ends, at = ([], 0)
    for a in arrays[:-1]:
        at += a.shape[along]
        ends.append(at)
    both = jnp.concatenate(arrays, axis=along)
    return tuple(jnp.split(lax.all_gather(both, axis, axis=dim, tiled=True), ends, axis=along))


def in_blocks(array, dim, size):
    lengths = array.shape
    tiles = array.reshape(*lengths[:dim], size, lengths[dim] // size, *lengths[dim + 1 :])
    return jnp.moveaxis(tiles, dim, 0)


def sum_at_owner(array, axis, dim):
    size = lax.axis_size(axis)
    tiles = lax.all_to_all(in_blocks(array, dim, size), axis, 0, 0, tiled=True)
    return jnp.sum(tiles.astype(jnp.float32), axis=0)


def joined_along(tiles, dim):
    tiles = jnp.moveaxis(tiles, 0, dim)
    lengths = tiles.shape
    return tiles.reshape(*lengths[:dim], lengths[dim] * lengths[dim + 1], *lengths[dim + 2 :])


def moved_by_axis(tiles, axes, sequence):
    lengths = [lax.axis_size(a) for a in axes]
    tiles = tiles.reshape(*lengths, *tiles.shape[1:])
    for k in sequence:
        tiles = lax.all_to_all(tiles, axes[k], split_axis=k, concat_axis=k, tiled=True)
    return tiles.reshape(-1, *tiles.shape[len(axes) :])


def two_step_exchange(array, groups, sequence, split_dim, concat_dim):
    size = lax.axis_size(groups[0]) * lax.axis_size(groups[1])
    tiles = in_blocks(array, split_dim, size)
    return joined_along(moved_by_axis(tiles, groups, sequence), concat_dim)


def normalize(entries, gain):
    wide = entries.astype(jnp.float32)
    factor = lax.rsqrt(jnp.mean(wide * wide, axis=-1, keepdims=True) + EPSILON)
    return wide * factor * gain.astype(jnp.float32)


def rotate(entries, positions):
    half = entries.shape[-1] // 2
    freqs = THETA ** (-jnp.arange(half, dtype=jnp.float32) / half)
    angle = positions.astype(jnp.float32)[:, None, None] * freqs[None, None, :]
    cosine = jnp.cos(angle)
    sine = jnp.sin(angle)
    first = entries[..., :half].astype(jnp.float32)
    second = entries[..., half:].astype(jnp.float32)
    turned = jnp.concatenate(
        [first * cosine - second * sine, first * sine + second * cosine], axis=-1
    )
    return turned.astype(jnp.bfloat16)


def rounded(entries):
    return lax.optimization_barrier(entries.astype(jnp.bfloat16)).astype(jnp.float32)


def attend(
    query_plain,
    query_rotary,
    latent_input,
    rotary_key,
    key_weight,
    value_weight,
    latent_gain,
    head_gain,
    out_weight,
):
    tokens = query_plain.shape[0]
    heads = key_weight.shape[1] // PLAIN_DIM
    offset = lax.axis_index(EP) * tokens
    positions = offset + jnp.arange(tokens, dtype=jnp.int32)
    last_position = offset + tokens - 1
    latent = normalize(latent_input, latent_gain).astype(jnp.bfloat16)
    key_rotated = rotate(rotary_key.reshape(tokens, 1, ROTARY_DIM), positions).reshape(
        tokens, ROTARY_DIM
    )
    query_rotated = rotate(query_rotary.reshape(tokens, heads, ROTARY_DIM), positions)
    queries = query_plain.reshape(tokens, heads, PLAIN_DIM)
    factor = (PLAIN_DIM + ROTARY_DIM) ** (-0.5)

    def reshape_given(piece):
        key_rows, value_rows, rotated_rows = piece
        count = key_rows.shape[0]
        return (
            key_rows.reshape(count, heads, PLAIN_DIM),
            value_rows.reshape(count, heads, VALUE_DIM),
            rotated_rows,
        )

    def add_keys(carry, unpacked, start):
        total, highest = carry
        keys, values, rotated_rows = unpacked
        count = keys.shape[0]
        scores = jnp.einsum("qhd,khd->qhk", queries, keys, preferred_element_type=jnp.float32)
        scores = scores + jnp.einsum(
            "qhr,kr->qhk", query_rotated, rotated_rows, preferred_element_type=jnp.float32
        )
        scores = scores * factor
        key_positions = start + jnp.arange(count, dtype=jnp.int32)
        allowed = (key_positions[None, :] <= positions[:, None])[:, None, :]
        masked = jnp.where(allowed, scores, -1e30)
        newest = jnp.maximum(highest, jnp.max(masked, axis=-1))
        weights = jnp.where(allowed, jnp.exp(masked - newest[..., None]), 0.0).astype(jnp.bfloat16)
        total = total * jnp.exp(highest - newest)[..., None] + jnp.einsum(
            "qhk,khd->qhd", weights, values, preferred_element_type=jnp.float32
        )
        return (total, newest)

    def make_fold(unpack):

        def guarded(carry, piece, start):

            def compute(state):
                return add_keys(state, unpack(piece), start)

            def keep(state):
                return state

            return lax.cond(start > last_position, keep, compute, carry)

        def fold(carry, piece, start):
            count = piece[0].shape[0]

            def step(index, inner):
                begin = index * key_span
                sliced = tuple(
                    (lax.dynamic_slice_in_dim(member, begin, key_span, 0) for member in piece)
                )
                return guarded(inner, sliced, begin)

            return lax.fori_loop(0, count // key_span, step, carry)

        return fold

    initial = (
        jnp.zeros((tokens, heads, VALUE_DIM), jnp.float32),
        jnp.full((tokens, heads), -1e30, jnp.float32),
    )
    own_keys = jnp.dot(latent, key_weight, preferred_element_type=jnp.float32).astype(jnp.bfloat16)
    own_values = jnp.dot(latent, value_weight, preferred_element_type=jnp.float32).astype(
        jnp.bfloat16
    )
    folded = make_fold(reshape_given)(
        initial, sent_together((own_keys, own_values, key_rotated), EP, 0, 1), jnp.int32(0)
    )
    context = folded[0]
    head_output = (
        normalize(context, head_gain.reshape(heads, VALUE_DIM))
        .astype(jnp.bfloat16)
        .reshape(tokens, heads * VALUE_DIM)
    )
    summed = sum_at_owner(
        rounded(jnp.dot(head_output, out_weight, preferred_element_type=jnp.float32)).astype(
            jnp.bfloat16
        ),
        "tp",
        0,
    )
    return summed.astype(jnp.bfloat16)


def experts(expert_input, expert_gain, routes, route_weight, gate_weight, up_weight, down_weight):
    tokens = expert_input.shape[0]
    features = expert_input.shape[1]
    count_ep = lax.axis_size(EP)
    capacity = min(tokens, max(2, (9 * tokens + 4 * count_ep - 1) // (4 * count_ep)))
    normed = normalize(expert_input, expert_gain).astype(jnp.bfloat16)
    chosen = routes.reshape(-1)
    onehot = (chosen[:, None] == jnp.arange(count_ep, dtype=jnp.int32)[None, :]).astype(jnp.int32)
    ranks = jnp.sum(jnp.cumsum(onehot, axis=0) * onehot, axis=1) - 1
    destination = chosen * capacity + ranks
    outgoing = (
        jnp.zeros((count_ep * capacity, features), jnp.bfloat16)
        .at[destination]
        .set(jnp.repeat(normed, TOP, axis=0))
    )
    gate_local = gate_weight[0]
    up_local = up_weight[0]
    down_local = down_weight[0]
    arrived = two_step_exchange(outgoing, ("ep_0", "ep_1"), (1, 0), 0, 0)
    piece = lax.all_gather(arrived, "tp", axis=0, tiled=True)
    gate = jnp.dot(piece, gate_local, preferred_element_type=jnp.float32)
    upward = jnp.dot(piece, up_local, preferred_element_type=jnp.float32)
    hidden = (jax.nn.silu(gate) * upward).astype(jnp.bfloat16)
    summed = sum_at_owner(
        rounded(jnp.dot(hidden, down_local, preferred_element_type=jnp.float32)).astype(
            jnp.bfloat16
        ),
        "tp",
        0,
    ).astype(jnp.bfloat16)
    returned = lax.all_to_all(summed, EP, split_axis=0, concat_axis=0, tiled=True)
    picked = returned[destination].astype(jnp.float32).reshape(tokens, TOP, features)
    combined = jnp.sum(picked * route_weight[:, :, None], axis=1)
    return combined.astype(jnp.bfloat16)


def body(
    query_plain,
    query_rotary,
    latent_input,
    rotary_key,
    key_weight,
    value_weight,
    latent_gain,
    head_gain,
    out_weight,
    expert_input,
    expert_gain,
    routes,
    route_weight,
    gate_weight,
    up_weight,
    down_weight,
):
    attended = attend(
        query_plain,
        query_rotary,
        latent_input,
        rotary_key,
        key_weight,
        value_weight,
        latent_gain,
        head_gain,
        out_weight,
    )
    expert_out = experts(
        expert_input, expert_gain, routes, route_weight, gate_weight, up_weight, down_weight
    )
    return (attended, expert_out)


def solution(mesh):
    finer = Mesh(
        mesh.devices.reshape(mesh.shape["grp"], 16, 2, mesh.shape["tp"]),
        ("grp", "ep_0", "ep_1", "tp"),
    )
    in_specs = (
        P(GRP_EP, "tp"),
        P(GRP_EP, "tp"),
        P(GRP_EP, None),
        P(GRP_EP, None),
        P(None, "tp"),
        P(None, "tp"),
        P(),
        P("tp"),
        P("tp", None),
        P(GRP_EP_TP, None),
        P(),
        P(GRP_EP_TP, None),
        P(GRP_EP_TP, None),
        P(EP, None, "tp"),
        P(EP, None, "tp"),
        P(EP, "tp", None),
    )
    out_specs = (P(GRP_EP_TP, None), P(GRP_EP_TP, None))
    return jax.shard_map(body, mesh=finer, in_specs=in_specs, out_specs=out_specs, check_vma=False)
```

profile of v0, /device:TPU:33, one launch (start us, length us, event | category | flops | bytes accessed | tf_op | source)
XLA Modules:
  0.0 412.7 jit_solution(7010274078072165320)
XLA Ops:
  7.2 0.0 copy-start
  7.2 0.1 all-gather.5.cloned.1.call-start
  7.3 0.8 copy.31
  8.1 0.1 eq.29
  8.2 0.1 eq.25
  8.4 0.7 broadcast_multiply_fusion
  9.1 0.6 reduce-window.6
  9.7 0.2 slice_reduce_fusion
  9.9 0.1 fusion.34
  10.0 0.1 copy.30
  10.1 0.1 mul.234
  10.2 0.7 convert_element_type.123
  10.9 1.2 fusion.19
  12.2 1.2 fusion.21
  13.4 0.6 broadcast_in_dim.62
  14.1 0.4 reshape.310
  14.5 3.2 scatter_custom_fusion
  17.7 1.6 reshape_reshape.6
  19.3 0.7 copy.34
  20.0 24.7 %all_to_all.32 = bf16[16,2,9,2048]{3,0,2,1:T(8,128)(2,1)S(1)} all-to-all(bf16[16,2,9,2048]{3,0,2,1:T(8,128)(2,1)S(1)} %copy.34), channel_id=1, replica_groups=mesh['grp'=2,'ep_0'=16,'ep_1'=2,'tp'=4] {'ep_1'}, dimensions={1} | all-to-all | bytes 2359296 | tf_op jit(solution)/shard_map/all_to_all | solution.py:50
  44.7 1.2 copy.35
  46.0 61.2 %all_to_all.33 = bf16[16,2,9,2048]{3,1,2,0:T(2,128)(2,1)S(1)} all-to-all(bf16[16,2,9,2048]{3,1,2,0:T(2,128)(2,1)S(1)} %copy.35), channel_id=1, replica_groups=mesh['grp'=2,'ep_0'=16,'ep_1'=2,'tp'=4] {'ep_0'}, dimensions={0} | all-to-all | bytes 2359296 | tf_op jit(solution)/shard_map/all_to_all | solution.py:50
  107.2 0.7 copy.36
  107.8 1.4 reshape_reshape.7
  109.2 0.1 all-gather.5.cloned.1.call-update
  109.3 0.2 all-gather.3.cloned.1.call-start
  109.6 0.1 fusion.24
  109.7 0.1 fusion.45
  109.9 0.3 convolution_convert_fusion.2
  110.2 0.3 convolution_convert_fusion.3
  110.5 0.7 pad_maximum_fusion
  111.1 0.1 all-gather.3.cloned.1.call-update
  111.2 53.7 %all-gather.5.cloned.1.call-done = bf16[1152,2048]{1,0:T(8,128)(2,1)} async-done(((bf16[288,2048]{1,0:T(8,128)(2,1)}), bf16[1152,2048]{1,0:T(8,128)(2,1)}) %all-gather.5.cloned.1.call-update) | async-done | bytes 4718608 | tf_op jit(solution)/shard_map/all_gather | solution.py:208
  164.9 8.1 %fusion.14 = f32[1152,896]{1,0:T(8,128)S(1)} fusion(bf16[1152,2048]{1,0:T(8,128)(2,1)} %all-gather.5.cloned.1.call-done, bf16[1,2048,896]{2,1,0:T(8,128)(2,1)} %param.33), kind=kOutput, calls=%fused_computation.25 | convolution fusion | flops 4227858432 | bytes 12517376 | tf_op jit(solution)/shard_map/dot_general | solution.py:209
  173.0 5.3 %fusion.16 = bf16[1152,896]{1,0:T(8,128)(2,1)S(1)} fusion(bf16[1152,2048]{1,0:T(8,128)(2,1)S(1)} %copy-done.6, bf16[1,2048,896]{2,1,0:T(8,128)(2,1)S(1)} %copy-done.7, f32[1152,896]{1,0:T(8,128)S(1)} %fusion.14), kind=kOutput, calls=%fused_computation.27 | convolution fusion | flops 4234051584 | bytes 14581760 | tf_op jit(solution)/shard_map/dot_general | solution.py:210
  178.4 6.8 %convolution_convert_fusion = bf16[1152,2048]{1,0:T(8,128)(2,1)} fusion(bf16[1152,896]{1,0:T(8,128)(2,1)S(1)} %fusion.16, bf16[1,896,2048]{2,1,0:T(8,128)(2,1)S(1)} %copy-done.8), kind=kOutput, calls=%fused_computation.21 | convolution fusion | flops 4230217728 | bytes 10452992 | tf_op jit(solution)/shard_map/dot_general | solution.py:213
  185.1 5.1 %all-to-all-start.3 = ((bf16[4,288,2048]{2,1,0:T(8,128)(2,1)}), bf16[4,288,2048]{2,1,0:T(8,128)(2,1)}, u32[]{:S(2)}, u32[]{:S(2)}) async-start(bf16[4,288,2048]{2,1,0:T(8,128)(2,1)} %bitcast.70), calls=%async_computation.3 | async-start | bytes 9437184 | tf_op jit(solution)/shard_map/all_to_all | solution.py:36
  190.3 0.1 copy.29
  190.4 0.1 reshape.296
  190.5 0.1 multiply_cosine_fusion
  190.7 57.7 %all-gather.3.cloned.1.call-done = bf16[8192,288]{0,1:T(8,128)(2,1)} async-done(((bf16[256,288]{0,1:T(8,128)(2,1)}), bf16[8192,288]{0,1:T(8,128)(2,1)}) %all-gather.3.cloned.1.call-update) | async-done | bytes 4718608 | tf_op jit(solution)/shard_map/all_gather | solution.py:25
  248.4 1.1 split.13
  249.5 3.9 fusion.47
  253.4 4.5 %while.16 = (s32[]{:T(128)}, f32[256,2,64]{0,2,1:T(8,128)S(1)}, f32[256,2]{0,1:T(2,128)S(1)}, s32[]{:T(128)}, bf16[8192,128]{0,1:T(8,128)(2,1)}, /*index=5*/bf16...) while((s32[]{:T(128)}, f32[256,2,64]{0,2,1:T(8,128)S(1)}, ...), condition=%wide.region_5.6_spmd.clone, body=%wide.region_1.5_spmd.clone.sunk | while | flops 343476992 | bytes 22022456 | solution.py:158
  253.4 4.3 %conditional.3 = ((f32[256,2,64]{0,2,1:T(8,128)S(1)}, f32[256,2]{0,1:T(2,128)S(1)})) conditional(s32[]{:T(128)} %convert_element_type.210, (s32[]{:T(128)}, s32[]{:T(128)}, bf16[8192,128]{0,1:T(8,128)(2,1)}, bf16[256,2,64]{0,2,1:T(8,128)(2,1)S(1)}, bf16[8192,32]{0,1:T(8,128)(2,1)S(1)}, /*index=5*/bf16[256,2,32]{0,2,1:T(8,128)(2,1)S(1)}, ...), branch_computations={%region_2.3_spmd, %region_4.4_spmd} | conditional | flops 343476992 | bytes 22021194 | solution.py:146
  253.5 1.1 constant_dynamic-slice_fusion
  254.6 0.8 fusion.48
  255.4 0.5 broadcast_compare_fusion
  255.8 1.1 fusion.46
  257.0 0.8 fusion.7
  258.0 0.1 multiply_convert_fusion
  258.1 1.4 convolution_convert_fusion.1
  259.5 3.7 all-to-all-start
  263.2 3.3 reduce_sum.74
  266.6 1.6 all_to_all.24
  268.2 9.7 %all-to-all-done = bf16[4,64,2048]{2,1,0:T(8,128)(2,1)S(1)} async-done(((bf16[4,64,2048]{2,1,0:T(8,128)(2,1)}), bf16[4,64,2048]{2,1,0:T(8,128)(2,1)S(1)}, u32[]{:S(2)}, u32[]{:S(2)}) %all-to-all-start) | async-done | bytes 1048608 | tf_op jit(solution)/shard_map/all_to_all | solution.py:36
  277.9 18.7 %all-to-all-start.4 = ((bf16[32,9,2048]{2,1,0:T(8,128)(2,1)}), bf16[32,9,2048]{2,1,0:T(8,128)(2,1)}, u32[]{:S(2)}, u32[]{:S(2)}) async-start(bf16[32,9,2048]{2,1,0:T(8,128)(2,1)} %all_to_all.24), calls=%async_computation.4 | async-start | bytes 4194304 | tf_op jit(solution)/shard_map/all_to_all | solution.py:219
  296.6 0.1 copy.37
  296.7 0.9 reduce_sum.71
  297.7 97.7 %all-to-all-done.4 = bf16[32,9,2048]{2,1,0:T(8,128)(2,1)} async-done(((bf16[32,9,2048]{2,1,0:T(8,128)(2,1)}), bf16[32,9,2048]{2,1,0:T(8,128)(2,1)}, u32[]{:S(2)}, u32[]{:S(2)}) %all-to-all-start.4) | async-done | bytes 1179680 | tf_op jit(solution)/shard_map/all_to_all | solution.py:219
  395.3 1.8 all_to_all.26
  397.2 2.3 gather_fusion
  399.5 2.4 reshape.297
  401.9 3.9 multiply_reduce_fusion
  (53 shorter events, 0.3 us)
Async XLA Ops:
  7.2 250.9 %copy-start = (bf16[128,2048]{1,0:T(8,128)(2,1)S(1)}, bf16[128,2048]{1,0:T(8,128)(2,1)}, u32[]{:S(2)}) copy-start(bf16[128,2048]{1,0:T(8,128)(2,1)} %param.28) | copy-start | bytes 1572868
  7.2 157.7 %all-gather.5.cloned.1.call-start = ((), (), s32[]{:S(2)}) async-start(), calls=%async_computation.6 | async-start | bytes 5898240 | tf_op jit(solution)/shard_map/all_gather | solution.py:208
  107.1 2.4 copy-start.11
  107.1 2.4 copy-start.1
  107.1 2.6 copy-start.4
  107.1 2.7 copy-start.9
  107.2 3.0 copy-start.10
  109.3 139.1 %all-gather.3.cloned.1.call-start = ((), (), s32[]{:S(2)}) async-start(), calls=%async_computation.5 | async-start | bytes 4866048 | tf_op jit(solution)/shard_map/all_gather | solution.py:25
  164.9 8.1 %copy-start.6 = (bf16[1152,2048]{1,0:T(8,128)(2,1)S(1)}, bf16[1152,2048]{1,0:T(8,128)(2,1)}, u32[]{:S(2)}) copy-start(bf16[1152,2048]{1,0:T(8,128)(2,1)} %all-gather.5.cloned.1.call-done) | copy-start | bytes 14155780
  164.9 8.1 %copy-start.7 = (bf16[1,2048,896]{2,1,0:T(8,128)(2,1)S(1)}, bf16[1,2048,896]{2,1,0:T(8,128)(2,1)}, u32[]{:S(2)}) copy-start(bf16[1,2048,896]{2,1,0:T(8,128)(2,1)} %param.34) | copy-start | bytes 11010052
  173.0 5.3 %copy-start.8 = (bf16[1,896,2048]{2,1,0:T(8,128)(2,1)S(1)}, bf16[1,896,2048]{2,1,0:T(8,128)(2,1)}, u32[]{:S(2)}) copy-start(bf16[1,896,2048]{2,1,0:T(8,128)(2,1)} %param.35) | copy-start | bytes 11010052
  185.1 5.2 %copy-start.2 = (bf16[256,128]{1,0:T(8,128)(2,1)S(1)}, bf16[256,128]{1,0:T(8,128)(2,1)}, u32[]{:S(2)}) copy-start(bf16[256,128]{1,0:T(8,128)(2,1)} %param.20) | copy-start | bytes 196612
  185.1 5.3 %copy-start.12 = (bf16[128]{0:T(256)(128)(2,1)S(1)}, bf16[128]{0:T(256)(128)(2,1)}, u32[]{:S(2)}) copy-start(bf16[128]{0:T(256)(128)(2,1)} %param.27) | copy-start | bytes 772
  185.1 5.5 %copy-start.3 = (bf16[256,64]{0,1:T(8,128)(2,1)S(1)}, bf16[256,64]{0,1:T(8,128)(2,1)}, u32[]{:S(2)}) copy-start(bf16[256,64]{0,1:T(8,128)(2,1)} %param.21) | copy-start | bytes 98308
  185.1 74.4 %all-to-all-start.3 = ((bf16[4,288,2048]{2,1,0:T(8,128)(2,1)}), bf16[4,288,2048]{2,1,0:T(8,128)(2,1)}, u32[]{:S(2)}, u32[]{:S(2)}) async-start(bf16[4,288,2048]{2,1,0:T(8,128)(2,1)} %bitcast.70), calls=%async_computation.3 | async-start | bytes 9437184 | tf_op jit(solution)/shard_map/all_to_all | solution.py:36
  259.5 18.3 %all-to-all-start = ((bf16[4,64,2048]{2,1,0:T(8,128)(2,1)}), bf16[4,64,2048]{2,1,0:T(8,128)(2,1)S(1)}, u32[]{:S(2)}, u32[]{:S(2)}) async-start(bf16[4,64,2048]{2,1,0:T(8,128)(2,1)} %bitcast.12), calls=%async_computation | async-start | bytes 2097152 | tf_op jit(solution)/shard_map/all_to_all | solution.py:36
  266.6 30.1 %copy-start.5 = (f32[128,2]{0,1:T(2,128)S(1)}, f32[128,2]{0,1:T(2,128)}, u32[]{:S(2)}) copy-start(f32[128,2]{0,1:T(2,128)} %param.32) | copy-start | bytes 3076
  277.9 117.5 %all-to-all-start.4 = ((bf16[32,9,2048]{2,1,0:T(8,128)(2,1)}), bf16[32,9,2048]{2,1,0:T(8,128)(2,1)}, u32[]{:S(2)}, u32[]{:S(2)}) async-start(bf16[32,9,2048]{2,1,0:T(8,128)(2,1)} %all_to_all.24), calls=%async_computation.4 | async-start | bytes 4194304 | tf_op jit(solution)/shard_map/all_to_all | solution.py:219
Sparse Core Ops, SparseCore 0:
  109.4 55.4 all-gather.4
  167.2 81.1 all-gather.2
where the time goes:
time: 414 us; the launch traced here: 413 us
  waiting for transfers between devices  219 us (53%)
  blocking collectives  85.9 us (21%)
  starting transfers between devices  27.9 us (7%)
  local copies, waits for them, and re-layouts  25.9 us (6%)
  matrix products  24.8 us (6%)
  other arithmetic  14.5 us (4%)
  between operations  14.5 us (4%)
    all_to_all x1, waiting for transfers between devices, experts(): lax.all_to_all(summed, EP, split_axis=0, concat_axis=0, tiled=True)  97.7 us
    all_to_all x2, blocking collectives, moved_by_axis(): lax.all_to_all(tiles, axes[k], split_axis=k, concat_axis=k, tiled=True)  85.9 us
    all_gather x1, waiting for transfers between devices, sent_together(): lax.all_gather(both, axis, axis=dim, tiled=True)  57.7 us
    all_gather x1, waiting for transfers between devices, experts(): piece = lax.all_gather(arrived, 'tp', axis=0, tiled=True)  53.7 us
    all_to_all x1, starting transfers between devices, experts(): lax.all_to_all(summed, EP, split_axis=0, concat_axis=0, tiled=True)  18.7 us
    all_to_all x2, waiting for transfers between devices, sum_at_owner(): tiles = lax.all_to_all(in_blocks(array, dim, size), axis, 0, 0, tiled=True)  9.7 us
    all_to_all x2, starting transfers between devices, sum_at_owner(): tiles = lax.all_to_all(in_blocks(array, dim, size), axis, 0, 0, tiled=True)  8.82 us
  transfers between devices with their start and end apart: 5, of which 4 were waited for; matrix products, arithmetic and copies ran while one was open for 9% of the time, Pallas kernels for 0%

commit v1 on v0

--- a/solution.py
+++ b/solution.py
@@ -14,6 +14,19 @@
 EPSILON = 1e-06
 THETA = 10000.0
 key_span = 2048
+
+
+def collect(x, axis, dim):
+    size, index, extent = (lax.axis_size(axis), lax.axis_index(axis), x.shape[dim])
+    ahead = [(i, (i + 1) % size) for i in range(size)]
+    out = jnp.zeros((*x.shape[:dim], size * extent, *x.shape[dim + 1 :]), x.dtype)
+    block = x
+    for step in range(size):
+        holder = (index - step) % size
+        out = lax.dynamic_update_slice_in_dim(out, block, holder * extent, axis=dim)
+        if step < size - 1:
+            block = lax.ppermute(block, axis, ahead)
+    return out
 
 
 def sent_together(arrays, axis, dim, along):
@@ -205,7 +218,7 @@
     up_local = up_weight[0]
     down_local = down_weight[0]
     arrived = two_step_exchange(outgoing, ("ep_0", "ep_1"), (1, 0), 0, 0)
-    piece = lax.all_gather(arrived, "tp", axis=0, tiled=True)
+    piece = collect(arrived, "tp", 0)
     gate = jnp.dot(piece, gate_local, preferred_element_type=jnp.float32)
     upward = jnp.dot(piece, up_local, preferred_element_type=jnp.float32)
     hidden = (jax.nn.silu(gate) * upward).astype(jnp.bfloat16)

time: 414 us -> 420 us (1.014)
  blocking collectives: 85.9 us -> 24.9 us
  waiting for transfers between devices: 219 us -> 261 us
  starting transfers between devices: 27.9 us -> 50.2 us
  local copies, waits for them, and re-layouts: 25.9 us -> 32.1 us
    ppermute x0 -> x3, waiting for transfers between devices: none -> 68.8 us  [collect(): block = lax.ppermute(block, axis, ahead)]
    all_to_all x2 -> x1, blocking collectives: 85.9 us -> 24.9 us  [moved_by_axis(): lax.all_to_all(tiles, axes[k], split_axis=k, concat_axis=k, tiled=True)]
    all_gather x1, waiting for transfers between devices: 57.7 us -> 0.02 us  [sent_together(): lax.all_gather(both, axis, axis=dim, tiled=True)]
    all_to_all x0 -> x1, waiting for transfers between devices: none -> 54.4 us  [moved_by_axis(): lax.all_to_all(tiles, axes[k], split_axis=k, concat_axis=k, tiled=True)]
    all_gather x1 -> x0, waiting for transfers between devices: 53.7 us -> none  [experts(): piece = lax.all_gather(arrived, 'tp', axis=0, tiled=True)]
    all_to_all x2, waiting for transfers between devices: 9.7 us -> 39.8 us  [sum_at_owner(): tiles = lax.all_to_all(in_blocks(array, dim, size), axis, 0, 0, tiled=True)]
    all_to_all x1, starting transfers between devices: 18.7 us -> 35 us  [experts(): lax.all_to_all(summed, EP, split_axis=0, concat_axis=0, tiled=True)]
    all_to_all x0 -> x1, starting transfers between devices: none -> 4.79 us  [moved_by_axis(): lax.all_to_all(tiles, axes[k], split_axis=k, concat_axis=k, tiled=True)]
  transfers between devices with their start and end apart: 5 -> 8, of which waited for: 4 -> 7; matrix products, arithmetic and copies ran while one was open for 9% -> 10% of each run, Pallas kernels for 0% -> 0%
where the time goes in v1:
time: 420 us; the launch traced here: 419 us
  waiting for transfers between devices  261 us (62%)
  starting transfers between devices  50.2 us (12%)
  local copies, waits for them, and re-layouts  32.1 us (8%)
  blocking collectives  24.9 us (6%)
  matrix products  21.8 us (5%)
  between operations  14.6 us (3%)
  other arithmetic  14.5 us (3%)
    all_to_all x1, waiting for transfers between devices, experts(): lax.all_to_all(summed, EP, split_axis=0, concat_axis=0, tiled=True)  97.7 us
    ppermute x3, waiting for transfers between devices, collect(): block = lax.ppermute(block, axis, ahead)  68.8 us
    all_to_all x1, waiting for transfers between devices, moved_by_axis(): lax.all_to_all(tiles, axes[k], split_axis=k, concat_axis=k, tiled=True)  54.4 us
    all_to_all x2, waiting for transfers between devices, sum_at_owner(): tiles = lax.all_to_all(in_blocks(array, dim, size), axis, 0, 0, tiled=True)  39.8 us
    all_to_all x1, starting transfers between devices, experts(): lax.all_to_all(summed, EP, split_axis=0, concat_axis=0, tiled=True)  35 us
    all_to_all x1, blocking collectives, moved_by_axis(): lax.all_to_all(tiles, axes[k], split_axis=k, concat_axis=k, tiled=True)  24.9 us
    all_to_all x2, starting transfers between devices, sum_at_owner(): tiles = lax.all_to_all(in_blocks(array, dim, size), axis, 0, 0, tiled=True)  9.01 us
  transfers between devices with their start and end apart: 8, of which 7 were waited for; matrix products, arithmetic and copies ran while one was open for 10% of the time, Pallas kernels for 0%

profile of v1, /device:TPU:33, one launch (start us, length us, event | category | flops | bytes accessed | tf_op | source)
XLA Modules:
  0.0 419.1 jit_solution(11127622951917714148)
XLA Ops:
  7.2 0.8 copy.31
  8.0 0.1 eq.34
  8.2 0.1 eq.30
  8.3 0.7 broadcast_multiply_fusion
  9.0 0.6 reduce-window.6
  9.6 0.2 slice_reduce_fusion
  9.9 0.1 copy.30
  10.0 0.1 mul.246
  10.2 0.7 convert_element_type.123
  10.9 1.2 fusion.19
  12.1 1.2 fusion.21
  13.4 0.6 broadcast_in_dim.66
  14.0 0.4 reshape.310
  14.5 3.2 scatter_custom_fusion
  17.7 1.6 reshape_reshape.6
  19.2 0.7 copy.34
  20.0 24.9 %all_to_all.32 = bf16[16,2,9,2048]{3,0,2,1:T(8,128)(2,1)S(1)} all-to-all(bf16[16,2,9,2048]{3,0,2,1:T(8,128)(2,1)S(1)} %copy.34), channel_id=1, replica_groups=mesh['grp'=2,'ep_0'=16,'ep_1'=2,'tp'=4] {'ep_1'}, dimensions={1} | all-to-all | bytes 2359296 | tf_op jit(solution)/shard_map/all_to_all | solution.py:63
  44.9 2.2 copy.35
  47.1 4.8 %all-to-all-start.2 = ((bf16[16,2,9,2048]{3,1,2,0:T(2,128)(2,1)}), bf16[16,2,9,2048]{3,1,2,0:T(2,128)(2,1)}, u32[]{:S(2)}, u32[]{:S(2)}) async-start(bf16[16,2,9,2048]{3,1,2,0:T(2,128)(2,1)} %copy.35), calls=%async_computation.2 | async-start | bytes 2359296 | tf_op jit(solution)/shard_map/all_to_all | solution.py:63
  52.1 0.1 fusion.24
  52.2 0.1 fusion.45
  52.4 0.3 convolution_convert_fusion.2
  52.6 0.3 convolution_convert_fusion.3
  52.9 0.7 pad_maximum_fusion
  53.7 54.4 %all-to-all-done.2 = bf16[16,2,9,2048]{3,1,2,0:T(2,128)(2,1)} async-done(((bf16[16,2,9,2048]{3,1,2,0:T(2,128)(2,1)}), bf16[16,2,9,2048]{3,1,2,0:T(2,128)(2,1)}, u32[]{:S(2)}, u32[]{:S(2)}) %all-to-all-start.2) | async-done | bytes 1179680 | tf_op jit(solution)/shard_map/all_to_all | solution.py:63
  108.1 1.9 copy.36
  110.0 1.4 reshape_reshape.7
  111.4 1.3 collective-permute-start
  112.7 22.4 %collective-permute-done = bf16[288,2048]{1,0:T(8,128)(2,1)S(1)} collective-permute-done((bf16[288,2048]{1,0:T(8,128)(2,1)}, bf16[288,2048]{1,0:T(8,128)(2,1)S(1)}, u32[]{:S(2)}, u32[]{:S(2)}) %collective-permute-start) | collective-permute-done | bytes 1179680 | tf_op jit(solution)/shard_map/ppermute | solution.py:28
  135.1 24.5 %collective-permute-done.1 = bf16[288,2048]{1,0:T(8,128)(2,1)} collective-permute-done((bf16[288,2048]{1,0:T(8,128)(2,1)S(1)}, bf16[288,2048]{1,0:T(8,128)(2,1)}, u32[]{:S(2)}, u32[]{:S(2)}) %collective-permute-start.1) | collective-permute-done | bytes 1179680 | tf_op jit(solution)/shard_map/ppermute | solution.py:28
  159.6 0.6 broadcast_in_dim.64
  160.2 0.1 constant_dynamic-update-slice_fusion.3
  160.4 0.1 constant_dynamic-update-slice_fusion.2
  160.5 1.6 constant_dynamic-update-slice_fusion.1
  162.1 22.0 %collective-permute-done.2 = bf16[288,2048]{1,0:T(8,128)(2,1)} collective-permute-done((bf16[288,2048]{1,0:T(8,128)(2,1)}, bf16[288,2048]{1,0:T(8,128)(2,1)}, u32[]{:S(2)}, u32[]{:S(2)}) %collective-permute-start.2) | collective-permute-done | bytes 1179680 | tf_op jit(solution)/shard_map/ppermute | solution.py:28
  184.1 1.4 constant_dynamic-update-slice_fusion
  185.5 5.1 %fusion.17 = f32[1152,896]{1,0:T(8,128)S(1)} fusion(bf16[1152,2048]{1,0:T(8,128)(2,1)S(1)} %constant_dynamic-update-slice_fusion, bf16[1,2048,896]{2,1,0:T(8,128)(2,1)S(1)} %copy-done.7), kind=kOutput, calls=%fused_computation.26 | convolution fusion | flops 4227858432 | bytes 12517376 | tf_op jit(solution)/shard_map/dot_general | solution.py:222
  190.6 5.3 %multiply_convert_fusion = bf16[1152,896]{1,0:T(8,128)(2,1)S(1)} fusion(f32[1152,896]{1,0:T(8,128)S(1)} %fusion.17, bf16[1152,2048]{1,0:T(8,128)(2,1)S(1)} %constant_dynamic-update-slice_fusion, bf16[1,2048,896]{2,1,0:T(8,128)(2,1)S(1)} %copy-done.8), kind=kOutput, calls=%fused_computation.22 | convolution fusion | flops 4234051584 | bytes 14581760 | tf_op jit(solution)/shard_map/dot_general | solution.py:223
  195.9 6.7 %convolution_convert_fusion = bf16[1152,2048]{1,0:T(8,128)(2,1)} fusion(bf16[1152,896]{1,0:T(8,128)(2,1)S(1)} %multiply_convert_fusion, bf16[1,896,2048]{2,1,0:T(8,128)(2,1)S(1)} %copy-done.9), kind=kOutput, calls=%fused_computation.21 | convolution fusion | flops 4230217728 | bytes 10452992 | tf_op jit(solution)/shard_map/dot_general | solution.py:226
  202.7 5.2 %all-to-all-start.3 = ((bf16[4,288,2048]{2,1,0:T(8,128)(2,1)}), bf16[4,288,2048]{2,1,0:T(8,128)(2,1)}, u32[]{:S(2)}, u32[]{:S(2)}) async-start(bf16[4,288,2048]{2,1,0:T(8,128)(2,1)} %bitcast.70), calls=%async_computation.3 | async-start | bytes 9437184 | tf_op jit(solution)/shard_map/all_to_all | solution.py:49
  208.1 0.1 multiply_cosine_fusion
  208.3 1.1 split.13
  209.4 3.9 fusion.47
  213.3 4.5 %while.16 = (s32[]{:T(128)}, f32[256,2,64]{0,2,1:T(8,128)S(1)}, f32[256,2]{0,1:T(2,128)S(1)}, s32[]{:T(128)}, bf16[8192,128]{0,1:T(8,128)(2,1)}, /*index=5*/bf16...) while((s32[]{:T(128)}, f32[256,2,64]{0,2,1:T(8,128)S(1)}, ...), condition=%wide.region_5.6_spmd.clone, body=%wide.region_1.5_spmd.clone.sunk | while | flops 343476992 | bytes 22022456 | solution.py:171
  213.4 4.3 %conditional.3 = ((f32[256,2,64]{0,2,1:T(8,128)S(1)}, f32[256,2]{0,1:T(2,128)S(1)})) conditional(s32[]{:T(128)} %convert_element_type.210, (s32[]{:T(128)}, s32[]{:T(128)}, bf16[8192,128]{0,1:T(8,128)(2,1)}, bf16[256,2,64]{0,2,1:T(8,128)(2,1)S(1)}, bf16[8192,32]{0,1:T(8,128)(2,1)S(1)}, /*index=5*/bf16[256,2,32]{0,2,1:T(8,128)(2,1)S(1)}, ...), branch_computations={%region_2.3_spmd, %region_4.4_spmd} | conditional | flops 343476992 | bytes 22021194 | solution.py:159
  213.4 1.1 constant_dynamic-slice_fusion
  214.5 0.8 fusion.48
  215.3 0.5 broadcast_compare_fusion
  215.8 1.1 fusion.46
  216.9 0.8 fusion.7
  218.0 1.4 convolution_convert_fusion.1
  219.5 34.9 %all-to-all-done.3 = bf16[4,288,2048]{2,1,0:T(8,128)(2,1)} async-done(((bf16[4,288,2048]{2,1,0:T(8,128)(2,1)}), bf16[4,288,2048]{2,1,0:T(8,128)(2,1)}, u32[]{:S(2)}, u32[]{:S(2)}) %all-to-all-start.3) | async-done | bytes 4718624 | tf_op jit(solution)/shard_map/all_to_all | solution.py:49
  254.3 3.8 all-to-all-start
  258.2 3.3 reduce_sum.74
  261.5 1.6 all_to_all.24
  263.1 5.0 %all-to-all-done = bf16[4,64,2048]{2,1,0:T(8,128)(2,1)S(1)} async-done(((bf16[4,64,2048]{2,1,0:T(8,128)(2,1)}), bf16[4,64,2048]{2,1,0:T(8,128)(2,1)S(1)}, u32[]{:S(2)}, u32[]{:S(2)}) %all-to-all-start) | async-done | bytes 1048608 | tf_op jit(solution)/shard_map/all_to_all | solution.py:49
  268.1 35.0 %all-to-all-start.4 = ((bf16[32,9,2048]{2,1,0:T(8,128)(2,1)}), bf16[32,9,2048]{2,1,0:T(8,128)(2,1)}, u32[]{:S(2)}, u32[]{:S(2)}) async-start(bf16[32,9,2048]{2,1,0:T(8,128)(2,1)} %all_to_all.24), calls=%async_computation.4 | async-start | bytes 4194304 | tf_op jit(solution)/shard_map/all_to_all | solution.py:232
  303.1 0.1 copy.37
  303.2 0.9 reduce_sum.71
  304.2 97.7 %all-to-all-done.4 = bf16[32,9,2048]{2,1,0:T(8,128)(2,1)} async-done(((bf16[32,9,2048]{2,1,0:T(8,128)(2,1)}), bf16[32,9,2048]{2,1,0:T(8,128)(2,1)}, u32[]{:S(2)}, u32[]{:S(2)}) %all-to-all-start.4) | async-done | bytes 1179680 | tf_op jit(solution)/shard_map/all_to_all | solution.py:232
  401.8 1.8 all_to_all.26
  403.7 2.3 gather_fusion
  406.0 2.4 reshape.297
  408.4 3.9 multiply_reduce_fusion
  (64 shorter events, 0.8 us)
Async XLA Ops:
  7.2 210.9 %copy-start = (bf16[128,2048]{1,0:T(8,128)(2,1)S(1)}, bf16[128,2048]{1,0:T(8,128)(2,1)}, u32[]{:S(2)}) copy-start(bf16[128,2048]{1,0:T(8,128)(2,1)} %param.28) | copy-start | bytes 1572868
  20.0 32.0 %copy-start.12 = (bf16[256]{0:T(256)(128)(2,1)S(1)}, bf16[256]{0:T(256)(128)(2,1)}, u32[]{:S(2)}) copy-start(bf16[256]{0:T(256)(128)(2,1)} %param.26) | copy-start | bytes 1540
  20.0 32.1 %copy-start.2 = (bf16[256,256]{1,0:T(8,128)(2,1)S(1)}, bf16[256,256]{1,0:T(8,128)(2,1)}, u32[]{:S(2)}) copy-start(bf16[256,256]{1,0:T(8,128)(2,1)} %param.22) | copy-start | bytes 393220
  20.0 32.2 %copy-start.5 = (bf16[256,32]{0,1:T(8,128)(2,1)S(1)}, bf16[256,32]{0,1:T(8,128)(2,1)}, u32[]{:S(2)}) copy-start(bf16[256,32]{0,1:T(8,128)(2,1)} %param.23) | copy-start | bytes 49156
  20.0 32.4 %copy-start.10 = (bf16[256,128]{1,0:T(8,128)(2,1)S(1)}, bf16[256,128]{1,0:T(8,128)(2,1)}, u32[]{:S(2)}) copy-start(bf16[256,128]{1,0:T(8,128)(2,1)} %param.25) | copy-start | bytes 196612
  20.0 32.6 %copy-start.11 = (bf16[256,128]{1,0:T(8,128)(2,1)S(1)}, bf16[256,128]{1,0:T(8,128)(2,1)}, u32[]{:S(2)}) copy-start(bf16[256,128]{1,0:T(8,128)(2,1)} %param.24) | copy-start | bytes 196612
  47.1 60.9 %all-to-all-start.2 = ((bf16[16,2,9,2048]{3,1,2,0:T(2,128)(2,1)}), bf16[16,2,9,2048]{3,1,2,0:T(2,128)(2,1)}, u32[]{:S(2)}, u32[]{:S(2)}) async-start(bf16[16,2,9,2048]{3,1,2,0:T(2,128)(2,1)} %copy.35), calls=%async_computation.2 | async-start | bytes 2359296 | tf_op jit(solution)/shard_map/all_to_all | solution.py:63
  51.9 156.4 %all-gather.2.cloned.1.call-start = ((), (), s32[]{:S(2)}) async-start(), calls=%async_computation.5 | async-start | bytes 4866048 | tf_op jit(solution)/shard_map/all_gather | solution.py:38
  111.4 48.8 %copy-start.1 = (bf16[288,2048]{1,0:T(8,128)(2,1)S(1)}, bf16[288,2048]{1,0:T(8,128)(2,1)}, u32[]{:S(2)}) copy-start(bf16[288,2048]{1,0:T(8,128)(2,1)} %reshape_reshape.7) | copy-start | bytes 3538948
  111.4 23.7 %collective-permute-start = (bf16[288,2048]{1,0:T(8,128)(2,1)}, bf16[288,2048]{1,0:T(8,128)(2,1)S(1)}, u32[]{:S(2)}, u32[]{:S(2)}) collective-permute-start(bf16[288,2048]{1,0:T(8,128)(2,1)} %reshape_reshape.7), channel_id=1, source_target_pairs={{0,1},{1,2},{2,3},{3,0},{4,5},{5,6},{6,7},{7,4},{8,9},{9,10},{10,1... | collective-permute-start | bytes 3538952 | tf_op jit(solution)/shard_map/ppermute | solution.py:28
  135.1 24.5 %collective-permute-start.1 = (bf16[288,2048]{1,0:T(8,128)(2,1)S(1)}, bf16[288,2048]{1,0:T(8,128)(2,1)}, u32[]{:S(2)}, u32[]{:S(2)}) collective-permute-start(bf16[288,2048]{1,0:T(8,128)(2,1)S(1)} %collective-permute-done), channel_id=1, source_target_pairs={{0,1},{1,2},{2,3},{3,0},{4,5},{5,6},{6,7},{7,4},{8,9},{9,10},{10,1... | collective-permute-start | bytes 3538952 | tf_op jit(solution)/shard_map/ppermute | solution.py:28
  159.6 24.4 %collective-permute-start.2 = (bf16[288,2048]{1,0:T(8,128)(2,1)}, bf16[288,2048]{1,0:T(8,128)(2,1)}, u32[]{:S(2)}, u32[]{:S(2)}) collective-permute-start(bf16[288,2048]{1,0:T(8,128)(2,1)} %collective-permute-done.1), channel_id=1, source_target_pairs={{0,1},{1,2},{2,3},{3,0},{4,5},{5,6},{6,7},{7,4},{8,9},{9,10},{10,1... | collective-permute-start | bytes 3538952 | tf_op jit(solution)/shard_map/ppermute | solution.py:28
  160.4 25.1 %copy-start.7 = (bf16[1,2048,896]{2,1,0:T(8,128)(2,1)S(1)}, bf16[1,2048,896]{2,1,0:T(8,128)(2,1)}, u32[]{:S(2)}) copy-start(bf16[1,2048,896]{2,1,0:T(8,128)(2,1)} %param.33) | copy-start | bytes 11010052
  185.5 5.1 %copy-start.8 = (bf16[1,2048,896]{2,1,0:T(8,128)(2,1)S(1)}, bf16[1,2048,896]{2,1,0:T(8,128)(2,1)}, u32[]{:S(2)}) copy-start(bf16[1,2048,896]{2,1,0:T(8,128)(2,1)} %param.34) | copy-start | bytes 11010052
  190.6 5.3 %copy-start.9 = (bf16[1,896,2048]{2,1,0:T(8,128)(2,1)S(1)}, bf16[1,896,2048]{2,1,0:T(8,128)(2,1)}, u32[]{:S(2)}) copy-start(bf16[1,896,2048]{2,1,0:T(8,128)(2,1)} %param.35) | copy-start | bytes 11010052
  202.7 5.2 %copy-start.3 = (bf16[256,128]{1,0:T(8,128)(2,1)S(1)}, bf16[256,128]{1,0:T(8,128)(2,1)}, u32[]{:S(2)}) copy-start(bf16[256,128]{1,0:T(8,128)(2,1)} %param.20) | copy-start | bytes 196612
  202.7 5.3 %copy-start.13 = (bf16[128]{0:T(256)(128)(2,1)S(1)}, bf16[128]{0:T(256)(128)(2,1)}, u32[]{:S(2)}) copy-start(bf16[128]{0:T(256)(128)(2,1)} %param.27) | copy-start | bytes 772
  202.7 5.6 %copy-start.4 = (bf16[256,64]{0,1:T(8,128)(2,1)S(1)}, bf16[256,64]{0,1:T(8,128)(2,1)}, u32[]{:S(2)}) copy-start(bf16[256,64]{0,1:T(8,128)(2,1)} %param.21) | copy-start | bytes 98308
  202.7 51.6 %all-to-all-start.3 = ((bf16[4,288,2048]{2,1,0:T(8,128)(2,1)}), bf16[4,288,2048]{2,1,0:T(8,128)(2,1)}, u32[]{:S(2)}, u32[]{:S(2)}) async-start(bf16[4,288,2048]{2,1,0:T(8,128)(2,1)} %bitcast.70), calls=%async_computation.3 | async-start | bytes 9437184 | tf_op jit(solution)/shard_map/all_to_all | solution.py:49
  254.3 13.7 %all-to-all-start = ((bf16[4,64,2048]{2,1,0:T(8,128)(2,1)}), bf16[4,64,2048]{2,1,0:T(8,128)(2,1)S(1)}, u32[]{:S(2)}, u32[]{:S(2)}) async-start(bf16[4,64,2048]{2,1,0:T(8,128)(2,1)} %bitcast.12), calls=%async_computation | async-start | bytes 2097152 | tf_op jit(solution)/shard_map/all_to_all | solution.py:49
  261.5 41.6 %copy-start.6 = (f32[128,2]{0,1:T(2,128)S(1)}, f32[128,2]{0,1:T(2,128)}, u32[]{:S(2)}) copy-start(f32[128,2]{0,1:T(2,128)} %param.32) | copy-start | bytes 3076
  268.1 133.7 %all-to-all-start.4 = ((bf16[32,9,2048]{2,1,0:T(8,128)(2,1)}), bf16[32,9,2048]{2,1,0:T(8,128)(2,1)}, u32[]{:S(2)}, u32[]{:S(2)}) async-start(bf16[32,9,2048]{2,1,0:T(8,128)(2,1)} %all_to_all.24), calls=%async_computation.4 | async-start | bytes 4194304 | tf_op jit(solution)/shard_map/all_to_all | solution.py:232
Sparse Core Ops, SparseCore 0:
  55.1 107.7 all-gather.1
